TPU v7x, 32 devices: a whole 2x2x4 slice. The times are simulated.
32 devices in a mesh: sp: 8 (over z, y), tp: 4 (over x, core).
Axes of the slice: x: 2, y: 2, z: 4, core: 2. Of those that a mesh axis runs over, the one named last changes fastest.
Arguments:
- queries_one: bfloat16 [2048, 512], P('sp', 'tp'), may hold values from -6 to 6
- queries_two: bfloat16 [2048, 512], P('sp', 'tp'), may hold values from -6 to 6
- keys_one: bfloat16 [2048, 512], P('sp', 'tp'), may hold values from -6 to 6
- keys_two: bfloat16 [2048, 512], P('sp', 'tp'), may hold values from -6 to 6
- values: bfloat16 [2048, 1024], P('sp', 'tp'), may hold values from -6 to 6
- mix_lambda: float32 [4], P('tp'), may hold values from 0.3 to 0.8
- head_gain: float32 [1024], P('tp'), may hold values from 0.1 to 1.9
- out_weight: bfloat16 [1024, 2048], P('tp'), may hold values from -0.1875 to 0.1875
- residual_in: bfloat16 [2048, 2048], P('sp', 'tp'), may hold values from -12 to 12
- norm_gain: float32 [2048], replicated, may hold values from 0.1 to 1.9
- gate_weight: bfloat16 [2048, 5632], P('sp', 'tp'), may hold values from -0.125 to 0.125
- up_weight: bfloat16 [2048, 5632], P('sp', 'tp'), may hold values from -0.125 to 0.125
- down_weight: bfloat16 [5632, 2048], P('tp', 'sp'), may hold values from -0.078125 to 0.078125
Outputs:
- layer_out: bfloat16 [2048, 2048], P('sp', 'tp')
All inputs are finite; a program needn't handle non-finite values.
Results may differ from a plain program's by a relative error of at most 0.012.
Values may be sent and summed in bfloat16 or wider, within the bound.
A program may use at most 192 MiB of HBM per device.

v0:
```python
import jax
import jax.numpy as jnp
from jax import lax
from jax.sharding import PartitionSpec as P

HEAD = 128
epsilon = 1e-06
masked_score = -1e30


def per_device(
    queries_one,
    queries_two,
    keys_one,
    keys_two,
    values,
    mix_lambda,
    head_gain,
    out_weight,
    residual_in,
    norm_gain,
    gate_weight,
    up_weight,
    down_weight,
):
    tok_rows = queries_one.shape[0]
    heads_here = mix_lambda.shape[0]
    head_width = HEAD
    value_width = values.shape[1] // heads_here
    query_pos = lax.axis_index("sp") * tok_rows + jnp.arange(tok_rows, dtype=jnp.int32)
    query_first = queries_one.reshape(tok_rows, heads_here, head_width)
    query_second = queries_two.reshape(tok_rows, heads_here, head_width)
    score_scale = head_width ** (-0.5)

    def update(state, queries, key_rows, value_rows, visible):
        running, totals, weighted = state
        scores = (
            jnp.einsum("qhd,khd->hqk", queries, key_rows, preferred_element_type=jnp.float32)
            * score_scale
        )
        scores = jnp.where(visible[None], scores, masked_score)
        highest = jnp.maximum(running, jnp.max(scores, axis=2))
        weights_exp = jnp.where(visible[None], jnp.exp(scores - highest[..., None]), 0.0)
        totals = jnp.sum(weights_exp, axis=2)
        weighted = jnp.einsum(
            "hqk,khd->hqd",
            weights_exp.astype(jnp.bfloat16),
            value_rows,
            preferred_element_type=jnp.float32,
        )
        return (highest, totals, weighted)

    initial = (
        jnp.full((heads_here, tok_rows), masked_score, jnp.float32),
        jnp.zeros((heads_here, tok_rows), jnp.float32),
        jnp.zeros((heads_here, tok_rows, value_width), jnp.float32),
    )
    key_first = lax.all_gather(keys_one, "sp", axis=0, tiled=True)
    key_second = lax.all_gather(keys_two, "sp", axis=0, tiled=True)
    value_piece = lax.all_gather(values, "sp", axis=0, tiled=True)
    key_count = key_first.shape[0]
    key_pos = jnp.arange(key_count, dtype=jnp.int32)
    visible = key_pos[None, :] <= query_pos[:, None]
    value_rows = value_piece.reshape(key_count, heads_here, value_width)
    first_new = update(
        initial,
        query_first,
        key_first.reshape(key_count, heads_here, head_width),
        value_rows,
        visible,
    )
    second_new = update(
        initial,
        query_second,
        key_second.reshape(key_count, heads_here, head_width),
        value_rows,
        visible,
    )
    lam_heads = mix_lambda[:, None, None]
    mixed = (
        first_new[2] / first_new[1][..., None]
        - lam_heads * second_new[2] / second_new[1][..., None]
    )
    mean_square = jnp.mean(mixed * mixed, axis=2, keepdims=True)
    normed_heads = (
        mixed
        * lax.rsqrt(mean_square + epsilon)
        * head_gain.reshape(heads_here, 1, value_width)
        * 0.8
    )
    attended = (
        normed_heads.transpose(1, 0, 2)
        .reshape(tok_rows, heads_here * value_width)
        .astype(jnp.bfloat16)
    )
    projected = lax.psum_scatter(
        lax.dot_general(
            out_weight, attended, (((0,), (1,)), ((), ())), preferred_element_type=jnp.float32
        ).astype(jnp.bfloat16),
        "tp",
        scatter_dimension=0,
        tiled=True,
    ).astype(jnp.float32)
    resid = (residual_in.astype(jnp.float32) + projected.T).astype(jnp.bfloat16)
    full_rows = lax.all_gather(resid, "tp", axis=1, tiled=True)
    full_float = full_rows.astype(jnp.float32)
    mean_rows = jnp.mean(full_float * full_float, axis=1, keepdims=True)
    normed = (full_float * lax.rsqrt(mean_rows + epsilon) * norm_gain[None, :]).astype(jnp.bfloat16)
    gate_act = jnp.dot(
        normed,
        lax.all_gather(gate_weight, "sp", axis=0, tiled=True),
        preferred_element_type=jnp.float32,
    )
    up_act = jnp.dot(
        normed,
        lax.all_gather(up_weight, "sp", axis=0, tiled=True),
        preferred_element_type=jnp.float32,
    )
    hidden = (jax.nn.silu(gate_act) * up_act).astype(jnp.bfloat16)
    partials = jnp.dot(
        hidden,
        lax.all_gather(down_weight, "sp", axis=1, tiled=True),
        preferred_element_type=jnp.float32,
    )
    mlp_out = lax.psum_scatter(
        partials.astype(jnp.bfloat16), "tp", scatter_dimension=1, tiled=True
    ).astype(jnp.float32)
    return (resid.astype(jnp.float32) + mlp_out).astype(jnp.bfloat16)


def solution(mesh):
    in_specs = (
        P("sp", "tp"),
        P("sp", "tp"),
        P("sp", "tp"),
        P("sp", "tp"),
        P("sp", "tp"),
        P("tp"),
        P("tp"),
        P("tp", None),
        P("sp", "tp"),
        P(),
        P("sp", "tp"),
        P("sp", "tp"),
        P("tp", "sp"),
    )
    out_specs = P("sp", "tp")
    return jax.shard_map(
        per_device, mesh=mesh, in_specs=in_specs, out_specs=out_specs, check_vma=False
    )
```

profile of v0, /device:TPU:0, one launch (start us, length us, event | category | flops | bytes accessed | tf_op | source)
XLA Modules:
  0.0 449.1 jit_solution(3199958501547778345)
XLA Ops:
  6.5 0.7 all-gather.6.cloned.1.call-update
  7.3 0.0 reduce-scatter.3.cloned.1.call-start
  8.0 33.5 %all_gather.23 = bf16[2048,128]{1,0:T(8,128)(2,1)S(1)} all-gather(bf16[256,128]{1,0:T(8,128)(2,1)} %param.16), channel_id=1, replica_groups=mesh['sp'=8,'tp'=4] {'sp'}, dimensions={0}, use_global_device_ids=true | all-gather | bytes 589824 | tf_op jit(solution)/shard_map/all_gather | solution.py:59
  41.5 1.4 fusion.34
  42.9 31.7 %all_gather.21 = bf16[2048,128]{1,0:T(8,128)(2,1)S(1)} all-gather(bf16[256,128]{1,0:T(8,128)(2,1)S(1)} %copy-done.5), channel_id=1, replica_groups=mesh['sp'=8,'tp'=4] {'sp'}, dimensions={0}, use_global_device_ids=true | all-gather | bytes 589824 | tf_op jit(solution)/shard_map/all_gather | solution.py:58
  74.6 0.6 fusion.33
  75.2 1.3 copy-done.2
  76.5 1.2 fusion.9
  77.7 0.0 all-gather.6.cloned.1.call-done
  77.7 2.7 convolution_divide_fusion
  80.5 0.8 multiply_reduce_fusion
  81.4 1.5 fusion.3
  82.9 0.0 reduce-scatter.3.cloned.1.call-update
  82.9 0.0 all-gather.8.cloned.1.call-start
  83.0 26.4 %reduce-scatter.3.cloned.1.call-done = bf16[512,256]{0,1:T(8,128)(2,1)} async-done(((bf16[2048,256]{0,1:T(8,128)(2,1)}), bf16[512,256]{0,1:T(8,128)(2,1)}) %reduce-scatter.3.cloned.1.call-update) | async-done | bytes 262160 | tf_op jit(solution)/shard_map/reduce_scatter | solution.py:96
  109.4 1.7 fusion.21
  111.1 0.0 all-gather.10.cloned.1.call-start
  111.1 0.5 all-gather.10.cloned.1.call-update
  111.7 0.0 all-gather.12.cloned.1.call-start
  111.7 0.5 all-gather.12.cloned.1.call-update
  112.3 0.0 all-gather.14.cloned.1.call-start
  112.3 0.5 all-gather.14.cloned.1.call-update
  112.8 0.0 reduce-scatter.5.cloned.1.call-start
  112.9 15.1 %all-gather.8.cloned.1.call-done = bf16[256,2048]{1,0:T(8,128)(2,1)} async-done(((bf16[256,512]{1,0:T(8,128)(2,1)}), bf16[256,2048]{1,0:T(8,128)(2,1)}) %all-gather.8.cloned.1.call-update) | async-done | bytes 1048592 | tf_op jit(solution)/shard_map/all_gather | solution.py:105
  128.0 1.5 fusion.4
  129.5 92.9 %all-gather.10.cloned.1.call-done = bf16[2048,1408]{1,0:T(8,128)(2,1)} async-done(((bf16[256,1408]{1,0:T(8,128)(2,1)}), bf16[2048,1408]{1,0:T(8,128)(2,1)}) %all-gather.10.cloned.1.call-update) | async-done | bytes 5767184 | tf_op jit(solution)/shard_map/all_gather | solution.py:111
  222.4 6.0 %fusion.24 = f32[256,1408]{1,0:T(8,128)} fusion(bf16[2048,1408]{1,0:T(8,128)(2,1)} %all-gather.10.cloned.1.call-done, bf16[256,2048]{1,0:T(8,128)(2,1)} %all-gather.8.cloned.1.call-done, f32[2048]{0:T(1024)S(1)} %copy-done.9, f32[256]{0:T(256)S(1)} %add_rsqrt_fusion), kind=kOutput, calls=%fused_computation.34 | convolution fusion | flops 1478492160 | bytes 8266752 | tf_op jit(solution)/shard_map/dot_general | solution.py:109
  228.3 86.6 %all-gather.12.cloned.1.call-done = bf16[2048,1408]{1,0:T(8,128)(2,1)} async-done(((bf16[256,1408]{1,0:T(8,128)(2,1)}), bf16[2048,1408]{1,0:T(8,128)(2,1)}) %all-gather.12.cloned.1.call-update) | async-done | bytes 5767184 | tf_op jit(solution)/shard_map/all_gather | solution.py:116
  314.9 93.2 %all-gather.14.cloned.1.call-done = bf16[1408,2048]{1,0:T(8,128)(2,1)} async-done(((bf16[1408,256]{1,0:T(8,128)(2,1)}), bf16[1408,2048]{1,0:T(8,128)(2,1)}) %all-gather.14.cloned.1.call-update) | async-done | bytes 5767184 | tf_op jit(solution)/shard_map/all_gather | solution.py:122
  408.2 9.3 %convolution_convert_fusion.1 = bf16[256,2048]{1,0:T(8,128)(2,1)} fusion(bf16[1408,2048]{1,0:T(8,128)(2,1)} %all-gather.14.cloned.1.call-done, bf16[2048,1408]{1,0:T(8,128)(2,1)} %all-gather.12.cloned.1.call-done, f32[256,1408]{1,0:T(8,128)} %fusion.24, bf16[256,2048]{1,0:T(8,128)(2,1)S(1)} %copy-done.3, f32[2048]{0:T(1024)S(1)} %copy-done.9, ...), kind=kOutput, calls=%fused_computation.9 | convolution fusion | flops 2957574144 | bytes 15082496 | tf_op jit(solution)/shard_map/dot_general | solution.py:120
  417.4 23.1 %reduce-scatter.5.cloned.1.call-done = bf16[256,512]{1,0:T(8,128)(2,1)} async-done(((bf16[256,2048]{1,0:T(8,128)(2,1)}), bf16[256,512]{1,0:T(8,128)(2,1)}) %reduce-scatter.5.cloned.1.call-update) | async-done | bytes 262160 | tf_op jit(solution)/shard_map/reduce_scatter | solution.py:125
  440.6 1.7 add_convert_fusion
  (27 shorter events, 0.1 us)
Async XLA Ops:
  6.5 74.8 %copy-start = (bf16[256,2048]{1,0:T(8,128)(2,1)S(1)}, bf16[256,2048]{1,0:T(8,128)(2,1)}, u32[]{:S(2)}) copy-start(bf16[256,2048]{1,0:T(8,128)(2,1)} %param.20) | copy-start | bytes 3145732
  6.5 36.4 %copy-start.5 = (bf16[256,128]{1,0:T(8,128)(2,1)S(1)}, bf16[256,128]{1,0:T(8,128)(2,1)}, u32[]{:S(2)}) copy-start(bf16[256,128]{1,0:T(8,128)(2,1)} %param.15) | copy-start | bytes 196612
  6.5 68.1 %copy-start.8 = (bf16[256,128]{1,0:T(8,128)(2,1)S(1)}, bf16[256,128]{1,0:T(8,128)(2,1)}, u32[]{:S(2)}) copy-start(bf16[256,128]{1,0:T(8,128)(2,1)} %param.13) | copy-start | bytes 196612
  6.5 71.2 %all-gather.6.cloned.1.call-start = ((), (), s32[]{:S(2)}) async-start(), calls=%async_computation.2 | async-start | bytes 1179648 | tf_op jit(solution)/shard_map/all_gather | solution.py:60
  7.3 102.1 %reduce-scatter.3.cloned.1.call-start = ((), (), s32[]{:S(2)}) async-start(), calls=%async_computation.3 | async-start | bytes 1310720 | tf_op jit(solution)/shard_map/reduce_scatter | solution.py:96
  75.2 1.3 copy-start.2
  77.7 2.7 copy-start.7
  80.5 0.9 copy-start.6
  81.3 28.1 %copy-start.4 = (bf16[256,512]{1,0:T(8,128)(2,1)S(1)}, bf16[256,512]{1,0:T(8,128)(2,1)}, u32[]{:S(2)}) copy-start(bf16[256,512]{1,0:T(8,128)(2,1)} %param.21) | copy-start | bytes 786436
  82.9 139.5 %copy-start.9 = (f32[2048]{0:T(1024)S(1)}, f32[2048]{0:T(1024)}, u32[]{:S(2)}) copy-start(f32[2048]{0:T(1024)} %param.22) | copy-start | bytes 24580
  82.9 45.1 %all-gather.8.cloned.1.call-start = ((), (), s32[]{:S(2)}) async-start(), calls=%async_computation.4 | async-start | bytes 1310720 | tf_op jit(solution)/shard_map/all_gather | solution.py:105
  111.1 111.3 %all-gather.10.cloned.1.call-start = ((), (), s32[]{:S(2)}) async-start(), calls=%async_computation.5 | async-start | bytes 6488064 | tf_op jit(solution)/shard_map/all_gather | solution.py:111
  111.7 203.2 %all-gather.12.cloned.1.call-start = ((), (), s32[]{:S(2)}) async-start(), calls=%async_computation.6 | async-start | bytes 6488064 | tf_op jit(solution)/shard_map/all_gather | solution.py:116
  112.3 295.9 %all-gather.14.cloned.1.call-start = ((), (), s32[]{:S(2)}) async-start(), calls=%async_computation.7 | async-start | bytes 6488064 | tf_op jit(solution)/shard_map/all_gather | solution.py:122
  112.8 327.7 %reduce-scatter.5.cloned.1.call-start = ((), (), s32[]{:S(2)}) async-start(), calls=%async_computation.8 | async-start | bytes 1310720 | tf_op jit(solution)/shard_map/reduce_scatter | solution.py:125
  129.5 278.7 %copy-start.3 = (bf16[256,2048]{1,0:T(8,128)(2,1)S(1)}, bf16[256,2048]{1,0:T(8,128)(2,1)}, u32[]{:S(2)}) copy-start(bf16[256,2048]{1,0:T(8,128)(2,1)} %all-gather.8.cloned.1.call-done) | copy-start | bytes 3145732
  228.3 212.3 %copy-start.1 = (bf16[256,512]{1,0:T(8,128)(2,1)S(1)}, bf16[256,512]{1,0:T(8,128)(2,1)}, u32[]{:S(2)}) copy-start(bf16[256,512]{1,0:T(8,128)(2,1)} %fusion.21) | copy-start | bytes 786436
Sparse Core Ops, SparseCore 0:
  9.5 44.7 all-gather.5
  83.0 26.2 reduce-scatter.2
  111.2 16.7 all-gather.7
  130.0 92.3 all-gather.9
  224.4 90.4 all-gather.11
  316.8 91.2 all-gather.13
  417.6 22.9 reduce-scatter.4
where the time goes:
time: 449 us
  waiting for transfers between devices  340 us (76%)
  blocking collectives  65.2 us (15%)
  matrix products  22.3 us (5%)
  between operations  14.3 us (3%)
  other arithmetic  6.13 us (1%)
    all_gather x1, waiting for transfers between devices, per_device(): lax.all_gather(down_weight, 'sp', axis=1, tiled=True)  93.2 us
    all_gather x1, waiting for transfers between devices, per_device(): lax.all_gather(gate_weight, 'sp', axis=0, tiled=True)  92.9 us
    all_gather x1, waiting for transfers between devices, per_device(): lax.all_gather(up_weight, 'sp', axis=0, tiled=True)  86.6 us
    all_gather x1, blocking collectives, per_device(): key_second = lax.all_gather(keys_two, 'sp', axis=0, tiled=True)  33.5 us
    all_gather x1, blocking collectives, per_device(): key_first = lax.all_gather(keys_one, 'sp', axis=0, tiled=True)  31.7 us
    reduce_scatter x1, waiting for transfers between devices, per_device(): lax.psum_scatter(lax.dot_general(out_weight, attended, (((0,), (1,)), (()...  26.4 us
    reduce_scatter x1, waiting for transfers between devices, per_device(): lax.psum_scatter(partials.astype(jnp.bfloat16), 'tp', scatter_dimension=1...  23.1 us
    all_gather x1, waiting for transfers between devices, per_device(): full_rows = lax.all_gather(resid, 'tp', axis=1, tiled=True)  15.1 us
  transfers between devices with their start and end apart: 7, of which 6 were waited for; matrix products, arithmetic and copies ran while one was open for 2% of the time, Pallas kernels for 0%

commit v1 on v0

--- a/solution.py
+++ b/solution.py
@@ -56,7 +56,12 @@
         jnp.zeros((heads_here, tok_rows, value_width), jnp.float32),
     )
     key_first = lax.all_gather(keys_one, "sp", axis=0, tiled=True)
-    key_second = lax.all_gather(keys_two, "sp", axis=0, tiled=True)
+    ring = [keys_two]
+    for hop in range(7):
+        ring.append(lax.ppermute(ring[-1], "sp", [(dev, (dev + 1) % 8) for dev in range(8)]))
+    key_second = jnp.roll(
+        jnp.concatenate(ring[::-1], axis=0), (lax.axis_index("sp") + 1) * ring[0].shape[0], axis=0
+    )
     value_piece = lax.all_gather(values, "sp", axis=0, tiled=True)
     key_count = key_first.shape[0]
     key_pos = jnp.arange(key_count, dtype=jnp.int32)

time: 449 us -> 459 us (1.022)
  waiting for transfers between devices: 340 us -> 372 us
  blocking collectives: 65.2 us -> 34.3 us
  starting transfers between devices: 0.24 us -> 5.05 us
    ppermute x0 -> x7, waiting for transfers between devices: none -> 36.5 us  [per_device(): lax.ppermute(ring[-1], 'sp', [(dev, (dev + 1) % 8) for dev in range(8)])]
    all_gather x1 -> x0, blocking collectives: 33.5 us -> none  [per_device(): key_second = lax.all_gather(keys_two, 'sp', axis=0, tiled=True)]
    ppermute x0 -> x7, starting transfers between devices: none -> 4.81 us  [per_device(): lax.ppermute(ring[-1], 'sp', [(dev, (dev + 1) % 8) for dev in range(8)])]
  transfers between devices with their start and end apart: 7 -> 14, of which waited for: 6 -> 12; matrix products, arithmetic and copies ran while one was open for 2% -> 3% of each run, Pallas kernels for 0% -> 0%
where the time goes in v1:
time: 459 us; the launch traced here: 458 us
  waiting for transfers between devices  372 us (81%)
  blocking collectives  34.3 us (7%)
  matrix products  22 us (5%)
  between operations  14.4 us (3%)
  other arithmetic  6.11 us (1%)
  starting transfers between devices  5.05 us (1%)
  local copies, waits for them, and re-layouts  4.95 us (1%)
    all_gather x1, waiting for transfers between devices, per_device(): lax.all_gather(down_weight, 'sp', axis=1, tiled=True)  93.2 us
    all_gather x1, waiting for transfers between devices, per_device(): lax.all_gather(gate_weight, 'sp', axis=0, tiled=True)  92.9 us
    all_gather x1, waiting for transfers between devices, per_device(): lax.all_gather(up_weight, 'sp', axis=0, tiled=True)  86.6 us
    ppermute x7, waiting for transfers between devices, per_device(): lax.ppermute(ring[-1], 'sp', [(dev, (dev + 1) % 8) for dev in range(8)])  36.5 us
    all_gather x1, blocking collectives, per_device(): key_first = lax.all_gather(keys_one, 'sp', axis=0, tiled=True)  34.3 us
    reduce_scatter x1, waiting for transfers between devices, per_device(): lax.psum_scatter(partials.astype(jnp.bfloat16), 'tp', scatter_dimension=1...  23.1 us
    reduce_scatter x1, waiting for transfers between devices, per_device(): lax.psum_scatter(lax.dot_general(out_weight, attended, (((0,), (1,)), (()...  22.5 us
    all_gather x1, waiting for transfers between devices, per_device(): full_rows = lax.all_gather(resid, 'tp', axis=1, tiled=True)  15.1 us
  transfers between devices with their start and end apart: 14, of which 12 were waited for; matrix products, arithmetic and copies ran while one was open for 3% of the time, Pallas kernels for 0%

profile of v1, /device:TPU:0, one launch (start us, length us, event | category | flops | bytes accessed | tf_op | source)
XLA Modules:
  0.0 458.3 jit_solution(8237977308402639834)
XLA Ops:
  6.5 3.0 collective-permute-start
  9.5 5.5 %collective-permute-done = bf16[256,128]{1,0:T(8,128)(2,1)S(1)} collective-permute-done((bf16[256,128]{1,0:T(8,128)(2,1)}, bf16[256,128]{1,0:T(8,128)(2,1)S(1)}, u32[]{:S(2)}, u32[]{:S(2)}) %collective-permute-start) | collective-permute-done | bytes 65568 | tf_op jit(solution)/shard_map/ppermute | solution.py:61
  15.0 7.0 %collective-permute-done.1 = bf16[256,128]{1,0:T(8,128)(2,1)S(1)} collective-permute-done((bf16[256,128]{1,0:T(8,128)(2,1)S(1)}, bf16[256,128]{1,0:T(8,128)(2,1)S(1)}, u32[]{:S(2)}, u32[]{:S(2)}) %collective-permute-start.1) | collective-permute-done | bytes 65568 | tf_op jit(solution)/shard_map/ppermute | solution.py:61
  22.0 7.0 %collective-permute-done.2 = bf16[256,128]{1,0:T(8,128)(2,1)S(1)} collective-permute-done((bf16[256,128]{1,0:T(8,128)(2,1)S(1)}, bf16[256,128]{1,0:T(8,128)(2,1)S(1)}, u32[]{:S(2)}, u32[]{:S(2)}) %collective-permute-start.2) | collective-permute-done | bytes 65568 | tf_op jit(solution)/shard_map/ppermute | solution.py:61
  29.0 6.9 %collective-permute-done.3 = bf16[256,128]{1,0:T(8,128)(2,1)S(1)} collective-permute-done((bf16[256,128]{1,0:T(8,128)(2,1)S(1)}, bf16[256,128]{1,0:T(8,128)(2,1)S(1)}, u32[]{:S(2)}, u32[]{:S(2)}) %collective-permute-start.3) | collective-permute-done | bytes 65568 | tf_op jit(solution)/shard_map/ppermute | solution.py:61
  35.9 34.3 %all_gather.18 = bf16[2048,128]{1,0:T(8,128)(2,1)} all-gather(bf16[256,128]{1,0:T(8,128)(2,1)} %param.15), channel_id=1, replica_groups=mesh['sp'=8,'tp'=4] {'sp'}, dimensions={0}, use_global_device_ids=true | all-gather | bytes 589824 | tf_op jit(solution)/shard_map/all_gather | solution.py:58
  70.2 1.8 collective-permute-start.5
  72.0 5.3 %collective-permute-done.5 = bf16[256,128]{1,0:T(8,128)(2,1)} collective-permute-done((bf16[256,128]{1,0:T(8,128)(2,1)S(1)}, bf16[256,128]{1,0:T(8,128)(2,1)}, u32[]{:S(2)}, u32[]{:S(2)}) %collective-permute-start.5) | collective-permute-done | bytes 65568 | tf_op jit(solution)/shard_map/ppermute | solution.py:61
  77.3 1.7 fusion.36
  79.6 4.9 %collective-permute-done.6 = bf16[256,128]{1,0:T(8,128)(2,1)} collective-permute-done((bf16[256,128]{1,0:T(8,128)(2,1)}, bf16[256,128]{1,0:T(8,128)(2,1)}, u32[]{:S(2)}, u32[]{:S(2)}) %collective-permute-start.6) | collective-permute-done | bytes 65568 | tf_op jit(solution)/shard_map/ppermute | solution.py:61
  84.6 0.8 constant_dynamic-update-slice_fusion.15
  85.4 0.9 constant_dynamic-update-slice_fusion.14
  86.4 0.9 constant_dynamic-update-slice_fusion.7
  87.3 0.9 constant_dynamic-update-slice_fusion.6
  88.2 0.6 fusion.37
  88.8 1.3 copy-done.2
  90.2 1.1 fusion.10
  91.4 2.2 convolution_divide_fusion
  93.5 0.8 multiply_reduce_fusion
  94.4 1.5 fusion.4
  96.0 22.5 %reduce-scatter.3.cloned.1.call-done = bf16[512,256]{0,1:T(8,128)(2,1)} async-done(((bf16[2048,256]{0,1:T(8,128)(2,1)}), bf16[512,256]{0,1:T(8,128)(2,1)}) %reduce-scatter.3.cloned.1.call-update) | async-done | bytes 262160 | tf_op jit(solution)/shard_map/reduce_scatter | solution.py:101
  118.5 1.7 fusion.22
  120.9 0.5 all-gather.12.cloned.1.call-update
  122.0 15.1 %all-gather.8.cloned.1.call-done = bf16[256,2048]{1,0:T(8,128)(2,1)} async-done(((bf16[256,512]{1,0:T(8,128)(2,1)}), bf16[256,2048]{1,0:T(8,128)(2,1)}) %all-gather.8.cloned.1.call-update) | async-done | bytes 1048592 | tf_op jit(solution)/shard_map/all_gather | solution.py:110
  137.1 1.5 fusion.5
  138.6 92.9 %all-gather.10.cloned.1.call-done = bf16[2048,1408]{1,0:T(8,128)(2,1)} async-done(((bf16[256,1408]{1,0:T(8,128)(2,1)}), bf16[2048,1408]{1,0:T(8,128)(2,1)}) %all-gather.10.cloned.1.call-update) | async-done | bytes 5767184 | tf_op jit(solution)/shard_map/all_gather | solution.py:116
  231.5 6.0 %fusion.26 = f32[256,1408]{1,0:T(8,128)} fusion(bf16[2048,1408]{1,0:T(8,128)(2,1)} %all-gather.10.cloned.1.call-done, bf16[256,2048]{1,0:T(8,128)(2,1)} %all-gather.8.cloned.1.call-done, f32[2048]{0:T(1024)S(1)} %copy-done.10, f32[256]{0:T(256)S(1)} %add_rsqrt_fusion), kind=kOutput, calls=%fused_computation.36 | convolution fusion | flops 1478492160 | bytes 8266752 | tf_op jit(solution)/shard_map/dot_general | solution.py:114
  237.5 86.6 %all-gather.12.cloned.1.call-done = bf16[2048,1408]{1,0:T(8,128)(2,1)} async-done(((bf16[256,1408]{1,0:T(8,128)(2,1)}), bf16[2048,1408]{1,0:T(8,128)(2,1)}) %all-gather.12.cloned.1.call-update) | async-done | bytes 5767184 | tf_op jit(solution)/shard_map/all_gather | solution.py:121
  324.1 93.2 %all-gather.14.cloned.1.call-done = bf16[1408,2048]{1,0:T(8,128)(2,1)} async-done(((bf16[1408,256]{1,0:T(8,128)(2,1)}), bf16[1408,2048]{1,0:T(8,128)(2,1)}) %all-gather.14.cloned.1.call-update) | async-done | bytes 5767184 | tf_op jit(solution)/shard_map/all_gather | solution.py:127
  417.3 9.3 %convolution_convert_fusion.1 = bf16[256,2048]{1,0:T(8,128)(2,1)} fusion(bf16[1408,2048]{1,0:T(8,128)(2,1)} %all-gather.14.cloned.1.call-done, bf16[2048,1408]{1,0:T(8,128)(2,1)} %all-gather.12.cloned.1.call-done, f32[256,1408]{1,0:T(8,128)} %fusion.26, bf16[256,2048]{1,0:T(8,128)(2,1)S(1)} %copy-done.4, f32[2048]{0:T(1024)S(1)} %copy-done.10, ...), kind=kOutput, calls=%fused_computation.10 | convolution fusion | flops 2957574144 | bytes 15082496 | tf_op jit(solution)/shard_map/dot_general | solution.py:125
  426.6 23.1 %reduce-scatter.5.cloned.1.call-done = bf16[256,512]{1,0:T(8,128)(2,1)} async-done(((bf16[256,2048]{1,0:T(8,128)(2,1)}), bf16[256,512]{1,0:T(8,128)(2,1)}) %reduce-scatter.5.cloned.1.call-update) | async-done | bytes 262160 | tf_op jit(solution)/shard_map/reduce_scatter | solution.py:130
  449.7 1.7 add_convert_fusion
  (57 shorter events, 1.6 us)
Async XLA Ops:
  6.5 87.9 %copy-start = (bf16[256,2048]{1,0:T(8,128)(2,1)S(1)}, bf16[256,2048]{1,0:T(8,128)(2,1)}, u32[]{:S(2)}) copy-start(bf16[256,2048]{1,0:T(8,128)(2,1)} %param.20) | copy-start | bytes 3145732
  6.5 84.8 %all-gather.6.cloned.1.call-start = ((), (), s32[]{:S(2)}) async-start(), calls=%async_computation.2 | async-start | bytes 1179648 | tf_op jit(solution)/shard_map/all_gather | solution.py:65
  6.5 8.5 %collective-permute-start = (bf16[256,128]{1,0:T(8,128)(2,1)}, bf16[256,128]{1,0:T(8,128)(2,1)S(1)}, u32[]{:S(2)}, u32[]{:S(2)}) collective-permute-start(bf16[256,128]{1,0:T(8,128)(2,1)} %param.16), channel_id=1, source_target_pairs={{0,4},{4,8},{8,12},{12,16},{16,20},{20,24},{24,28},{28,0},{1,5},{5... | collective-permute-start | bytes 196616 | tf_op jit(solution)/shard_map/ppermute | solution.py:61
  15.0 7.0 %collective-permute-start.1 = (bf16[256,128]{1,0:T(8,128)(2,1)S(1)}, bf16[256,128]{1,0:T(8,128)(2,1)S(1)}, u32[]{:S(2)}, u32[]{:S(2)}) collective-permute-start(bf16[256,128]{1,0:T(8,128)(2,1)S(1)} %collective-permute-done), channel_id=1, source_target_pairs={{0,4},{4,8},{8,12},{12,16},{16,20},{20,24},{24,28},{28,0},{1,5},{5... | collective-permute-start | bytes 196616 | tf_op jit(solution)/shard_map/ppermute | solution.py:61
  22.0 7.0 %collective-permute-start.2 = (bf16[256,128]{1,0:T(8,128)(2,1)S(1)}, bf16[256,128]{1,0:T(8,128)(2,1)S(1)}, u32[]{:S(2)}, u32[]{:S(2)}) collective-permute-start(bf16[256,128]{1,0:T(8,128)(2,1)S(1)} %collective-permute-done.1), channel_id=1, source_target_pairs={{0,4},{4,8},{8,12},{12,16},{16,20},{20,24},{24,28},{28,0},{1,5},{5... | collective-permute-start | bytes 196616 | tf_op jit(solution)/shard_map/ppermute | solution.py:61
  29.0 7.0 %collective-permute-start.3 = (bf16[256,128]{1,0:T(8,128)(2,1)S(1)}, bf16[256,128]{1,0:T(8,128)(2,1)S(1)}, u32[]{:S(2)}, u32[]{:S(2)}) collective-permute-start(bf16[256,128]{1,0:T(8,128)(2,1)S(1)} %collective-permute-done.2), channel_id=1, source_target_pairs={{0,4},{4,8},{8,12},{12,16},{16,20},{20,24},{24,28},{28,0},{1,5},{5... | collective-permute-start | bytes 196616 | tf_op jit(solution)/shard_map/ppermute | solution.py:61
  29.0 57.4 %copy-start.6 = (bf16[256,128]{1,0:T(8,128)(2,1)S(1)}, bf16[256,128]{1,0:T(8,128)(2,1)}, u32[]{:S(2)}) copy-start(bf16[256,128]{1,0:T(8,128)(2,1)} %param.16) | copy-start | bytes 196612
  29.0 89.5 %reduce-scatter.3.cloned.1.call-start = ((), (), s32[]{:S(2)}) async-start(), calls=%async_computation.3 | async-start | bytes 1310720 | tf_op jit(solution)/shard_map/reduce_scatter | solution.py:101
  35.9 34.3 %collective-permute-start.4 = (bf16[256,128]{1,0:T(8,128)(2,1)S(1)}, bf16[256,128]{1,0:T(8,128)(2,1)S(1)}, u32[]{:S(2)}, u32[]{:S(2)}) collective-permute-start(bf16[256,128]{1,0:T(8,128)(2,1)S(1)} %collective-permute-done.3), channel_id=1, source_target_pairs={{0,4},{4,8},{8,12},{12,16},{16,20},{20,24},{24,28},{28,0},{1,5},{5... | collective-permute-start | bytes 196616 | tf_op jit(solution)/shard_map/ppermute | solution.py:61
  70.2 7.1 %collective-permute-start.5 = (bf16[256,128]{1,0:T(8,128)(2,1)S(1)}, bf16[256,128]{1,0:T(8,128)(2,1)}, u32[]{:S(2)}, u32[]{:S(2)}) collective-permute-start(bf16[256,128]{1,0:T(8,128)(2,1)S(1)} %collective-permute-done.4), channel_id=1, source_target_pairs={{0,4},{4,8},{8,12},{12,16},{16,20},{20,24},{24,28},{28,0},{1,5},{5... | collective-permute-start | bytes 196616 | tf_op jit(solution)/shard_map/ppermute | solution.py:61
  77.3 7.3 %collective-permute-start.6 = (bf16[256,128]{1,0:T(8,128)(2,1)}, bf16[256,128]{1,0:T(8,128)(2,1)}, u32[]{:S(2)}, u32[]{:S(2)}) collective-permute-start(bf16[256,128]{1,0:T(8,128)(2,1)} %collective-permute-done.5), channel_id=1, source_target_pairs={{0,4},{4,8},{8,12},{12,16},{16,20},{20,24},{24,28},{28,0},{1,5},{5... | collective-permute-start | bytes 196616 | tf_op jit(solution)/shard_map/ppermute | solution.py:61
  79.6 8.6 %copy-start.9 = (bf16[256,128]{1,0:T(8,128)(2,1)S(1)}, bf16[256,128]{1,0:T(8,128)(2,1)}, u32[]{:S(2)}) copy-start(bf16[256,128]{1,0:T(8,128)(2,1)} %param.14) | copy-start | bytes 196612
  88.8 1.3 copy-start.2
  91.3 2.2 copy-start.3
  91.3 2.2 copy-start.8
  93.5 0.9 copy-start.7
  94.4 24.1 %copy-start.5 = (bf16[256,512]{1,0:T(8,128)(2,1)S(1)}, bf16[256,512]{1,0:T(8,128)(2,1)}, u32[]{:S(2)}) copy-start(bf16[256,512]{1,0:T(8,128)(2,1)} %param.21) | copy-start | bytes 786436
  96.0 135.5 %copy-start.10 = (f32[2048]{0:T(1024)S(1)}, f32[2048]{0:T(1024)}, u32[]{:S(2)}) copy-start(f32[2048]{0:T(1024)} %param.22) | copy-start | bytes 24580
  96.0 41.1 %all-gather.8.cloned.1.call-start = ((), (), s32[]{:S(2)}) async-start(), calls=%async_computation.4 | async-start | bytes 1310720 | tf_op jit(solution)/shard_map/all_gather | solution.py:110
  120.3 111.2 %all-gather.10.cloned.1.call-start = ((), (), s32[]{:S(2)}) async-start(), calls=%async_computation.5 | async-start | bytes 6488064 | tf_op jit(solution)/shard_map/all_gather | solution.py:116
  120.8 203.2 %all-gather.12.cloned.1.call-start = ((), (), s32[]{:S(2)}) async-start(), calls=%async_computation.6 | async-start | bytes 6488064 | tf_op jit(solution)/shard_map/all_gather | solution.py:121
  121.4 295.9 %all-gather.14.cloned.1.call-start = ((), (), s32[]{:S(2)}) async-start(), calls=%async_computation.7 | async-start | bytes 6488064 | tf_op jit(solution)/shard_map/all_gather | solution.py:127
  122.0 327.7 %reduce-scatter.5.cloned.1.call-start = ((), (), s32[]{:S(2)}) async-start(), calls=%async_computation.8 | async-start | bytes 1310720 | tf_op jit(solution)/shard_map/reduce_scatter | solution.py:130
  138.6 278.7 %copy-start.4 = (bf16[256,2048]{1,0:T(8,128)(2,1)S(1)}, bf16[256,2048]{1,0:T(8,128)(2,1)}, u32[]{:S(2)}) copy-start(bf16[256,2048]{1,0:T(8,128)(2,1)} %all-gather.8.cloned.1.call-done) | copy-start | bytes 3145732
  237.5 212.3 %copy-start.1 = (bf16[256,512]{1,0:T(8,128)(2,1)S(1)}, bf16[256,512]{1,0:T(8,128)(2,1)}, u32[]{:S(2)}) copy-start(bf16[256,512]{1,0:T(8,128)(2,1)} %fusion.22) | copy-start | bytes 786436
Sparse Core Ops, SparseCore 0:
  29.1 44.1 all-gather.5
  96.1 22.3 reduce-scatter.2
  120.4 16.6 all-gather.7
  139.2 92.3 all-gather.9
  233.5 90.4 all-gather.11
  326.0 91.2 all-gather.13
  426.7 22.9 reduce-scatter.4
